TPU v7x, 32 devices: a whole 2x2x4 slice. The times are simulated.
32 devices in a mesh: sp: 16 (over z, y, x), tp: 2 (over core).
Axes of the slice: x: 2, y: 2, z: 4, core: 2. Of those that a mesh axis runs over, the one named last changes fastest.
Arguments:
- latent: bfloat16 [4096, 2048], P(('sp', 'tp')), may hold values from -6 to 6
- condition: bfloat16 [2048], P('sp'), may hold values from -6 to 6
- context_condition: bfloat16 [2048], P('sp'), may hold values from -6 to 6
- context: bfloat16 [512, 2048], P('sp'), may hold values from -6 to 6
- w_shift: bfloat16 [2048, 2048], P('sp', 'tp'), may hold values from -0.125 to 0.125
- w_scale: bfloat16 [2048, 2048], P('sp', 'tp'), may hold values from -0.125 to 0.125
- w_gate: bfloat16 [2048, 2048], P('sp', 'tp'), may hold values from -0.125 to 0.125
- pre_gain: float32 [2048], replicated, may hold values from 0.1 to 1.9
- post_gain: float32 [2048], replicated, may hold values from 0.1 to 1.9
- query_gain: float32 [128], replicated, may hold values from 0.1 to 5
- key_gain: float32 [128], replicated, may hold values from 0.1 to 5
- w_query: bfloat16 [2048, 2048], P(None, 'tp'), may hold values from -0.125 to 0.125
- w_key: bfloat16 [2048, 1024], P(None, 'tp'), may hold values from -0.125 to 0.125
- w_value: bfloat16 [2048, 1024], P(None, 'tp'), may hold values from -0.125 to 0.125
- w_out: bfloat16 [2048, 2048], P('tp'), may hold values from -0.125 to 0.125
Outputs:
- updated: bfloat16 [4096, 2048], P(('sp', 'tp'))
All inputs are finite; a program needn't handle non-finite values.
Results may differ from a plain program's by a relative error of at most 0.0085.
The roundings to bfloat16 on the way count: a program that leaves them out, or rounds other values in their place, can miss the bound.
Values may be sent and summed in bfloat16 or wider, within the bound.
A program may use at most 64 MiB of HBM per device.

v0:
```python
import math

import jax
import jax.numpy as jnp
from jax import lax
from jax.sharding import PartitionSpec as P

GRID_W = 64


def rms(values, gain):
    values = values.astype(jnp.float32)
    return values * lax.rsqrt(jnp.mean(values * values, axis=-1, keepdims=True) + 1e-06) * gain


def rotate_grid(values, positions, grid_width):
    head_dim = values.shape[-1]
    half = head_dim // 2
    quarter = head_dim // 4
    freqs = 10000.0 ** (-jnp.arange(0, half, 2).astype(jnp.float32) / half)
    row_pos = (positions // grid_width).astype(jnp.float32)
    col_pos = (positions % grid_width).astype(jnp.float32)
    pieces = []
    for axis_pos, base in ((row_pos, 0), (col_pos, half)):
        angle = axis_pos[:, None, None] * freqs
        cosine = jnp.cos(angle)
        sine = jnp.sin(angle)
        first = values[..., base : base + quarter]
        second = values[..., base + quarter : base + half]
        pieces = pieces + [first * cosine - second * sine, second * cosine + first * sine]
    return jnp.concatenate(pieces, axis=-1)


def absorb(carry, grouped_query, key_rows, value_rows, offsets, head_dim):
    largest, total, summed = carry
    kv_dev = grouped_query.shape[1]
    key_heads = key_rows.reshape(key_rows.shape[0], kv_dev, head_dim)
    value_heads = value_rows.reshape(value_rows.shape[0], kv_dev, head_dim)
    scores = jnp.einsum(
        "tkgd,skd->kgts", grouped_query, key_heads, preferred_element_type=jnp.float32
    )
    scores = scores * head_dim ** (-0.5) + offsets
    new_largest = jnp.maximum(largest, jnp.max(scores, axis=-1))
    correction = jnp.exp(largest - new_largest)
    terms = jnp.exp(scores - new_largest[..., None])
    total = total * correction + jnp.sum(terms, axis=-1)
    summed = summed * correction[..., None] + jnp.einsum(
        "kgts,skd->kgtd",
        terms.astype(jnp.bfloat16),
        value_heads,
        preferred_element_type=jnp.float32,
    )
    return (new_largest, total, summed)


def absorb_blocks(carry, grouped_query, key_rows, value_rows, offsets, shard_rows, head_dim):
    length = key_rows.shape[0]
    size = length
    shards = length // shard_rows
    factor = 1
    for candidate in range(shards, 0, -1):
        if shards % candidate == 0 and candidate * shard_rows <= 2048:
            factor = candidate
            break
    size = factor * shard_rows
    blocks = length // size
    if blocks == 1:
        return absorb(carry, grouped_query, key_rows, value_rows, offsets, head_dim)

    def step_block(state, inputs):
        return (absorb(state, grouped_query, inputs[0], inputs[1], inputs[2], head_dim), None)

    width = key_rows.shape[1]
    stacked = (
        key_rows.reshape(blocks, size, width),
        value_rows.reshape(blocks, size, width),
        offsets.reshape(blocks, size),
    )
    carry, unused = lax.scan(step_block, carry, stacked)
    return carry


def body(
    latent,
    condition,
    context_condition,
    context,
    w_shift,
    w_scale,
    w_gate,
    pre_gain,
    post_gain,
    query_gain,
    key_gain,
    w_query,
    w_key,
    w_value,
    w_out,
):
    sp_count = lax.axis_size("sp")
    tp_count = lax.axis_size("tp")
    head_dim = query_gain.shape[0]
    heads_dev = w_query.shape[1] // head_dim
    kv_dev = w_key.shape[1] // head_dim
    group = heads_dev // kv_dev
    query_width = w_query.shape[1]
    key_width = w_key.shape[1]
    conds = jax.nn.silu(jnp.stack([condition, context_condition]).astype(jnp.float32)).astype(
        jnp.bfloat16
    )
    partial_mod = tuple(
        (
            jnp.dot(conds, weight, preferred_element_type=jnp.float32)
            for weight in (w_shift, w_scale, w_gate)
        )
    )
    partial_mod = lax.psum(partial_mod, "sp")
    shift, scale, gate = lax.all_gather(partial_mod, "tp", axis=1, tiled=True)
    normed = (rms(latent, pre_gain) * (1.0 + scale[0]) + shift[0]).astype(jnp.bfloat16)
    normed_context = (rms(context, pre_gain) * (1.0 + scale[1]) + shift[1]).astype(jnp.bfloat16)
    tok_dev = latent.shape[0] * tp_count
    ctx_dev = context.shape[0]
    weights_all = jnp.concatenate([w_query, w_key, w_value], axis=1)
    projected = jnp.dot(
        lax.all_gather(normed, "tp", axis=0, tiled=True),
        weights_all,
        preferred_element_type=jnp.float32,
    )
    positions = lax.axis_index("sp") * tok_dev + jnp.arange(tok_dev)
    query = projected[:, :query_width].reshape(tok_dev, heads_dev, head_dim)
    query = rotate_grid(rms(query, query_gain), positions, GRID_W).astype(jnp.bfloat16)
    key = projected[:, query_width : query_width + key_width].reshape(tok_dev, kv_dev, head_dim)
    key = (
        rotate_grid(rms(key, key_gain), positions, GRID_W)
        .astype(jnp.bfloat16)
        .reshape(tok_dev, key_width)
    )
    value = projected[:, query_width + key_width :].astype(jnp.bfloat16)
    grouped_query = query.reshape(tok_dev, kv_dev, group, head_dim)
    weights_kv = jnp.concatenate([w_key, w_value], axis=1)
    lift = math.log(tok_dev * sp_count / (4.0 * ctx_dev * sp_count))
    carry = (
        jnp.full((kv_dev, group, tok_dev), -1e30, jnp.float32),
        jnp.zeros((kv_dev, group, tok_dev), jnp.float32),
        jnp.zeros((kv_dev, group, tok_dev, head_dim), jnp.float32),
    )
    both = jnp.dot(normed_context, weights_kv, preferred_element_type=jnp.float32)
    context_key = rms(
        both[:, :key_width].reshape(normed_context.shape[0], kv_dev, head_dim), key_gain
    )
    context_key = context_key.astype(jnp.bfloat16).reshape(normed_context.shape[0], key_width)
    context_key, context_value = (context_key, both[:, key_width:].astype(jnp.bfloat16))
    context_key, context_value = (
        lax.all_gather(context_key, "sp", axis=0, tiled=True),
        lax.all_gather(context_value, "sp", axis=0, tiled=True),
    )
    context_offsets = jnp.full((context_key.shape[0],), lift, jnp.float32)
    carry = absorb_blocks(
        carry,
        grouped_query,
        context_key,
        context_value,
        context_offsets,
        context_key.shape[0],
        head_dim,
    )
    segments = (
        lax.all_gather(key, "sp", axis=0, tiled=True),
        lax.all_gather(value, "sp", axis=0, tiled=True),
    )
    length = segments[0].shape[0]
    within = jnp.arange(length) % tok_dev
    offsets = jnp.where(within >= tok_dev, lift, 0.0).astype(jnp.float32)
    largest, total, summed = absorb_blocks(
        carry, grouped_query, segments[0], segments[1], offsets, tok_dev, head_dim
    )
    attended = (
        (summed / total[..., None]).transpose(2, 0, 1, 3).reshape(tok_dev, heads_dev * head_dim)
    )
    attended = attended.astype(jnp.bfloat16)
    mixed = lax.psum_scatter(
        jnp.dot(attended, w_out, preferred_element_type=jnp.float32).astype(jnp.bfloat16),
        "tp",
        scatter_dimension=0,
        tiled=True,
    ).astype(jnp.float32)
    updated = latent.astype(jnp.float32) + gate[0] * rms(mixed, post_gain)
    return updated.astype(jnp.bfloat16)


def solution(mesh):
    placed = (
        P(("sp", "tp"), None),
        P("sp"),
        P("sp"),
        P("sp", None),
        P("sp", "tp"),
        P("sp", "tp"),
        P("sp", "tp"),
        P(),
        P(),
        P(),
        P(),
        P(None, "tp"),
        P(None, "tp"),
        P(None, "tp"),
        P("tp", None),
    )
    return jax.shard_map(
        body, mesh=mesh, in_specs=placed, out_specs=P(("sp", "tp"), None), check_vma=False
    )
```

profile of v0, /device:TPU:1, one launch (start us, length us, event | category | flops | bytes accessed | tf_op | source)
XLA Modules:
  0.0 348.8 jit_solution(15623858519975927511)
XLA Ops:
  6.5 1.3 fusion.33
  7.8 0.8 fusion.68
  8.7 1.1 fusion.66
  9.8 1.1 fusion.70
  10.9 63.7 %all-reduce = (f32[2,1024]{1,0:T(2,128)S(1)}, f32[2,1024]{1,0:T(2,128)S(1)}, f32[2,1024]{1,0:T(2,128)}) all-reduce(f32[2,1024]{1,0:T(2,128)S(1)} %fusion.66, f32[2,1024]{1,0:T(2,128)S(1)} %fusion.68, f32[2,1024]{1,0:T(2,128)S(1)} %fusion.70), channel_id=1, replica_groups=mesh['sp'=16,'tp'=2] {'sp'}, use_global_device_ids=true, to_apply=%region_3.4 | all-reduce | flops 6144 | bytes 49152 | tf_op jit(solution)/shard_map/psum | solution.py:117
  74.7 16.4 %all_gather.26 = f32[2,2048]{1,0:T(2,128)S(1)} all-gather(f32[2,1024]{1,0:T(2,128)S(1)} %get-tuple-element.98), channel_id=1, replica_groups=mesh['sp'=16,'tp'=2] {'tp'}, dimensions={1}, use_global_device_ids=true | all-gather | bytes 24576 | tf_op jit(solution)/shard_map/all_gather | solution.py:118
  91.0 1.8 all_gather.25
  92.9 2.1 fusion.37
  95.0 0.0 all-gather.8.cloned.1.call-start
  95.0 5.1 %all-gather.4.cloned.1.call-done = bf16[256,2048]{1,0:T(8,128)(2,1)} async-done(((bf16[128,2048]{1,0:T(8,128)(2,1)}), bf16[256,2048]{1,0:T(8,128)(2,1)}) %all-gather.4.cloned.1.call-update) | async-done | bytes 1048592 | tf_op jit(solution)/shard_map/all_gather | solution.py:125
  100.2 7.1 %fusion.9 = f32[256,2048]{1,0:T(8,128)S(1)} fusion(bf16[256,2048]{1,0:T(8,128)(2,1)} %all-gather.4.cloned.1.call-done, bf16[2048,512]{1,0:T(8,128)(2,1)} %param.30, bf16[2048,512]{1,0:T(8,128)(2,1)} %param.29, bf16[2048,1024]{1,0:T(8,128)(2,1)} %param.28), kind=kOutput, calls=%fused_computation.14 | convolution fusion | flops 2172649472 | bytes 11534336 | tf_op jit(solution)/shard_map/dot_general | solution.py:124
  107.3 0.9 slice.115
  108.3 1.6 multiply_cosine_fusion.1
  109.9 0.2 reshape.270
  110.1 0.3 multiply_reduce_fusion.1
  110.5 1.0 multiply_multiply_fusion.1
  111.5 1.8 subtract_convert_fusion.3
  113.3 0.8 pad_maximum_fusion.1
  114.1 0.7 copy.109
  114.9 0.0 reduce-scatter.2.cloned.1.call-start
  114.9 0.1 fusion.42
  115.1 3.1 fusion.15
  118.3 0.1 reduce_sum.73
  118.4 0.1 mul.380
  118.5 39.2 %all_gather.27 = bf16[512,512]{1,0:T(8,128)(2,1)S(1)} all-gather(bf16[32,512]{1,0:T(8,128)(2,1)S(1)} %fusion.53), channel_id=1, replica_groups=mesh['sp'=16,'tp'=2] {'sp'}, dimensions={0}, use_global_device_ids=true | all-gather | bytes 557056 | tf_op jit(solution)/shard_map/all_gather | solution.py:154
  157.8 0.1 reshape.267
  157.9 37.0 %all_gather.29 = bf16[512,512]{1,0:T(8,128)(2,1)S(1)} all-gather(bf16[32,512]{1,0:T(8,128)(2,1)S(1)} %slice.116), channel_id=1, replica_groups=mesh['sp'=16,'tp'=2] {'sp'}, dimensions={0}, use_global_device_ids=true | all-gather | bytes 557056 | tf_op jit(solution)/shard_map/all_gather | solution.py:155
  195.0 0.1 reshape.269
  195.1 1.4 slice_bitcast_fusion
  196.5 0.2 copy.98
  196.7 0.3 multiply_reduce_fusion
  197.1 0.1 copy.67
  197.1 0.1 copy.68
  197.3 0.3 multiply_multiply_fusion
  197.6 0.9 subtract_convert_fusion.1
  198.5 0.1 copy.69
  198.6 0.1 copy.70
  198.7 0.1 copy.72
  198.8 0.1 copy.71
  198.8 0.7 pad_maximum_fusion
  199.5 0.8 bitcast_reduce_fusion.1
  200.3 0.8 fusion.21
  201.2 2.4 fusion.27
  203.6 65.7 %all-gather.6.cloned.1.call-done = bf16[4096,512]{1,0:T(8,128)(2,1)} async-done(((bf16[256,512]{1,0:T(8,128)(2,1)}), bf16[4096,512]{1,0:T(8,128)(2,1)}) %all-gather.6.cloned.1.call-update) | async-done | bytes 4194320 | tf_op jit(solution)/shard_map/all_gather | solution.py:168
  269.3 54.2 %while.14 = (s32[]{:T(128)}, f32[4,2,256]{2,1,0:T(2,128)S(1)}, f32[4,2,256]{2,1,0:T(2,128)S(1)}, f32[4,2,256,128]{3,2,1,0:T(8,128)}, bf16[2,2048,512]{2,1,0:T(8,...) while((s32[]{:T(128)}, f32[4,2,256]{2,1,0:T(2,128)S(1)}, ...), condition=%wide.region_13.14_spmd, body=%wide.region_10.13_spmd.sunk | while | flops 2194149376 | bytes 82485384 | solution.py:79
  269.3 4.5 %constant_dynamic-slice_fusion.6 = (bf16[1,2048,512]{2,1,0:T(8,128)(2,1)}, bf16[1,2048,512]{2,1,0:T(8,128)(2,1)}) fusion(bf16[2,2048,512]{2,1,0:T(8,128)(2,1)} %get-tuple-element.225, s32[]{:T(128)S(6)} %copy.118, bf16[2,2048,512]{2,1,0:T(8,128)(2,1)} %get-tuple-element.222), kind=kLoop, calls=%fused_computation.10.clone.1 | loop fusion | bytes 8388612 | tf_op jit(solution)/shard_map/while/body/jit(dynamic_index_in_dim)/dynamic_slice | solution.py:79
  273.8 2.9 copy.112
  276.7 3.9 %copy.113 = bf16[1,2048,512]{1,2,0:T(8,128)(2,1)} copy(bf16[1,2048,512]{2,1,0:T(8,128)(2,1)} %get-tuple-element.199) | data formatting | bytes 4194304 | tf_op jit(solution)/shard_map/while/body/jit(dynamic_index_in_dim)/dynamic_slice | solution.py:79
  280.6 4.2 %bitcast_reduce_fusion.3 = (f32[4,2,256]{2,1,0:T(2,128)S(1)}, f32[4,2048,256,2]{2,1,3,0:T(8,128)S(1)}) fusion(f32[2048]{0:T(1024)S(1)} %bitcast.121, bf16[2048,4,128,1]{0,2,3,1:T(8,128)(2,1)S(1)} %bitcast.116, bf16[256,4,2,128]{3,0,2,1:T(8,128)(2,1)S(1)} %get-tuple-element.223), kind=kOutput, calls=%fused_computation.1.clone.1 | convolution fusion | flops 1086322688 | bytes 19415040 | tf_op jit(solution)/shard_map/while/body/eval_jaxpr/tkgd,skd->kgts/dot_general | solution.py:39
  284.8 4.2 %fusion.93 = f32[4,2,256]{2,1,0:T(2,128)S(1)} fusion(f32[4,2048,256,2]{2,1,3,0:T(8,128)S(1)} %get-tuple-element.196, f32[4,2,256]{2,1,0:T(2,128)S(1)} %max.4, f32[2048]{0:T(1024)S(1)} %bitcast.122), kind=kLoop, calls=%fused_computation.5.clone.1 | loop fusion | flops 16775168 | bytes 16801792 | tf_op jit(solution)/shard_map/while/body/eval_jaxpr/reduce_sum | solution.py:46
  289.1 7.3 %fusion.94 = f32[4,2,256,128]{3,2,1,0:T(8,128)} fusion(bf16[2048,4,128,1]{0,2,3,1:T(8,128)(2,1)S(1)} %bitcast.117, f32[4,2048,256,2]{2,1,3,0:T(8,128)S(1)} %get-tuple-element.196, f32[4,2,256]{2,1,0:T(2,128)S(1)} %max.4, f32[2048]{0:T(1024)S(1)} %bitcast.123, f32[4,2,256,128]{3,2,1,0:T(8,128)} %get-tuple-element.212, f32[4,2,256]{2,1,0:T(2,128)S(1)} %bitcast.139), kind=kOutput, calls=%fused_computation.7.clone.1 | convolution fusion | flops 1091043328 | bytes 20996096 | tf_op jit(solution)/shard_map/while/body/eval_jaxpr/kgts,skd->kgtd/dot_general | solution.py:47
  296.4 4.5 %constant_dynamic-slice_fusion.6 = (bf16[1,2048,512]{2,1,0:T(8,128)(2,1)}, bf16[1,2048,512]{2,1,0:T(8,128)(2,1)}) fusion(bf16[2,2048,512]{2,1,0:T(8,128)(2,1)} %get-tuple-element.225, s32[]{:T(128)S(6)} %copy.118, bf16[2,2048,512]{2,1,0:T(8,128)(2,1)} %get-tuple-element.222), kind=kLoop, calls=%fused_computation.10.clone.1 | loop fusion | bytes 8388612 | tf_op jit(solution)/shard_map/while/body/jit(dynamic_index_in_dim)/dynamic_slice | solution.py:79
  300.8 2.9 copy.112
  303.8 3.9 %copy.113 = bf16[1,2048,512]{1,2,0:T(8,128)(2,1)} copy(bf16[1,2048,512]{2,1,0:T(8,128)(2,1)} %get-tuple-element.199) | data formatting | bytes 4194304 | tf_op jit(solution)/shard_map/while/body/jit(dynamic_index_in_dim)/dynamic_slice | solution.py:79
  307.7 4.2 %bitcast_reduce_fusion.3 = (f32[4,2,256]{2,1,0:T(2,128)S(1)}, f32[4,2048,256,2]{2,1,3,0:T(8,128)S(1)}) fusion(f32[2048]{0:T(1024)S(1)} %bitcast.121, bf16[2048,4,128,1]{0,2,3,1:T(8,128)(2,1)S(1)} %bitcast.116, bf16[256,4,2,128]{3,0,2,1:T(8,128)(2,1)S(1)} %get-tuple-element.223), kind=kOutput, calls=%fused_computation.1.clone.1 | convolution fusion | flops 1086322688 | bytes 19415040 | tf_op jit(solution)/shard_map/while/body/eval_jaxpr/tkgd,skd->kgts/dot_general | solution.py:39
  311.9 4.2 %fusion.93 = f32[4,2,256]{2,1,0:T(2,128)S(1)} fusion(f32[4,2048,256,2]{2,1,3,0:T(8,128)S(1)} %get-tuple-element.196, f32[4,2,256]{2,1,0:T(2,128)S(1)} %max.4, f32[2048]{0:T(1024)S(1)} %bitcast.122), kind=kLoop, calls=%fused_computation.5.clone.1 | loop fusion | flops 16775168 | bytes 16801792 | tf_op jit(solution)/shard_map/while/body/eval_jaxpr/reduce_sum | solution.py:46
  316.2 7.3 %fusion.94 = f32[4,2,256,128]{3,2,1,0:T(8,128)} fusion(bf16[2048,4,128,1]{0,2,3,1:T(8,128)(2,1)S(1)} %bitcast.117, f32[4,2048,256,2]{2,1,3,0:T(8,128)S(1)} %get-tuple-element.196, f32[4,2,256]{2,1,0:T(2,128)S(1)} %max.4, f32[2048]{0:T(1024)S(1)} %bitcast.123, f32[4,2,256,128]{3,2,1,0:T(8,128)} %get-tuple-element.212, f32[4,2,256]{2,1,0:T(2,128)S(1)} %bitcast.139), kind=kOutput, calls=%fused_computation.7.clone.1 | convolution fusion | flops 1091043328 | bytes 20996096 | tf_op jit(solution)/shard_map/while/body/eval_jaxpr/kgts,skd->kgtd/dot_general | solution.py:47
  323.5 1.6 copy.80
  325.0 0.1 divide_convert_fusion
  325.2 4.5 %convolution_convert_fusion = bf16[256,2048]{1,0:T(8,128)(2,1)} fusion(bf16[256,1024]{0,1:T(8,128)(2,1)S(1)} %bitcast.134, bf16[1024,2048]{1,0:T(8,128)(2,1)} %param.31), kind=kOutput, calls=%fused_computation.30 | convolution fusion | flops 1074266112 | bytes 5767168 | tf_op jit(solution)/shard_map/dot_general | solution.py:182
  329.7 3.8 %all_gather.24 = f32[2,2048]{1,0:T(2,128)S(1)} all-gather(f32[2,1024]{1,0:T(2,128)S(1)} %copy-done.9), channel_id=1, replica_groups=mesh['sp'=16,'tp'=2] {'tp'}, dimensions={1}, use_global_device_ids=true | all-gather | bytes 24576 | tf_op jit(solution)/shard_map/all_gather | solution.py:118
  333.5 5.4 %reduce-scatter.2.cloned.1.call-done = bf16[128,2048]{1,0:T(8,128)(2,1)} async-done(((bf16[256,2048]{1,0:T(8,128)(2,1)}), bf16[128,2048]{1,0:T(8,128)(2,1)}) %reduce-scatter.2.cloned.1.call-update) | async-done | bytes 524304 | tf_op jit(solution)/shard_map/reduce_scatter | solution.py:181
  338.9 1.2 fusion.30
  340.2 2.1 fusion.38
  (61 shorter events, 0.5 us)
Async XLA Ops:
  6.5 1.3 copy-start
  6.5 93.6 %all-gather.4.cloned.1.call-start = ((), (), s32[]{:S(2)}) async-start(), calls=%async_computation.1 | async-start | bytes 1572864 | tf_op jit(solution)/shard_map/all_gather | solution.py:125
  95.0 108.6 %all-gather.8.cloned.1.call-start = ((), (), s32[]{:S(2)}) async-start(), calls=%async_computation.3 | async-start | bytes 4456448 | tf_op jit(solution)/shard_map/all_gather | solution.py:169
  107.3 6.0 %copy-start.4 = (f32[256,2048]{1,0:T(8,128)}, f32[256,2048]{1,0:T(8,128)S(1)}, u32[]{:S(2)}) copy-start(f32[256,2048]{1,0:T(8,128)S(1)} %fusion.9) | copy-start | bytes 6291460
  108.2 161.1 %all-gather.6.cloned.1.call-start = ((), (), s32[]{:S(2)}) async-start(), calls=%async_computation.2 | async-start | bytes 4456448 | tf_op jit(solution)/shard_map/all_gather | solution.py:168
  110.1 4.9 %copy-start.6 = (bf16[32,2048]{1,0:T(8,128)(2,1)S(1)}, bf16[32,2048]{1,0:T(8,128)(2,1)}, u32[]{:S(2)}) copy-start(bf16[32,2048]{1,0:T(8,128)(2,1)} %param.20) | copy-start | bytes 393220
  110.1 5.0 %copy-start.7 = (f32[2048]{0:T(1024)S(1)}, f32[2048]{0:T(1024)}, u32[]{:S(2)}) copy-start(f32[2048]{0:T(1024)} %param.24) | copy-start | bytes 24580
  114.1 4.3 %copy-start.10 = (f32[128]{0:T(128)S(1)}, f32[128]{0:T(128)}, u32[]{:S(2)}) copy-start(f32[128]{0:T(128)} %param.27) | copy-start | bytes 1540
  114.9 224.0 %reduce-scatter.2.cloned.1.call-start = ((), (), s32[]{:S(2)}) async-start(), calls=%async_computation.4 | async-start | bytes 1572864 | tf_op jit(solution)/shard_map/reduce_scatter | solution.py:181
  157.8 39.5 %copy-start.11 = (f32[128]{0:T(128)S(1)}, f32[128]{0:T(128)}, u32[]{:S(2)}) copy-start(f32[128]{0:T(128)} %param.26) | copy-start | bytes 1540
  195.1 2.5 copy-start.5
  284.8 4.3 %copy-start.2 = (bf16[1,2048,512]{1,2,0:T(8,128)(2,1)S(1)}, bf16[1,2048,512]{1,2,0:T(8,128)(2,1)}, u32[]{:S(2)}) copy-start(bf16[1,2048,512]{1,2,0:T(8,128)(2,1)} %copy.113) | copy-start | bytes 6291460 | tf_op jit(solution)/shard_map/while
  311.9 4.3 %copy-start.2 = (bf16[1,2048,512]{1,2,0:T(8,128)(2,1)S(1)}, bf16[1,2048,512]{1,2,0:T(8,128)(2,1)}, u32[]{:S(2)}) copy-start(bf16[1,2048,512]{1,2,0:T(8,128)(2,1)} %copy.113) | copy-start | bytes 6291460 | tf_op jit(solution)/shard_map/while
  325.1 4.6 %copy-start.9 = (f32[2,1024]{1,0:T(2,128)S(1)}, f32[2,1024]{1,0:T(2,128)}, u32[]{:S(2)}) copy-start(f32[2,1024]{1,0:T(2,128)} %get-tuple-element.100) | copy-start | bytes 24580
  325.1 17.2 %copy-start.1 = (bf16[128,1024]{1,0:T(8,128)(2,1)S(1)}, bf16[128,1024]{1,0:T(8,128)(2,1)}, u32[]{:S(2)}) copy-start(bf16[128,1024]{1,0:T(8,128)(2,1)} %param.22) | copy-start | bytes 786436
  325.1 15.0 %copy-start.3 = (bf16[128,2048]{1,0:T(8,128)(2,1)S(1)}, bf16[128,2048]{1,0:T(8,128)(2,1)}, u32[]{:S(2)}) copy-start(bf16[128,2048]{1,0:T(8,128)(2,1)} %param.17) | copy-start | bytes 1572868
  325.2 15.0 %copy-start.8 = (f32[2048]{0:T(1024)S(1)}, f32[2048]{0:T(1024)}, u32[]{:S(2)}) copy-start(f32[2048]{0:T(1024)} %param.25) | copy-start | bytes 24580
Sparse Core Ops, SparseCore 0:
  95.1 4.9 all-gather.3
  108.3 84.8 all-gather.7
  196.0 73.2 all-gather.5
  329.8 9.0 reduce-scatter.1
where the time goes:
time: 350 us; the launch traced here: 349 us
  blocking collectives  162 us (46%)
  waiting for transfers between devices  76.3 us (22%)
  matrix products  43.9 us (13%)
  local copies, waits for them, and re-layouts  28.5 us (8%)
  other arithmetic  24.4 us (7%)
  between operations  13.5 us (4%)
    all_gather x1, waiting for transfers between devices, body(): lax.all_gather(key, 'sp', axis=0, tiled=True)  65.7 us
    psum x1, blocking collectives, body(): partial_mod = lax.psum(partial_mod, 'sp')  63.7 us
    all_gather x1, blocking collectives, body(): lax.all_gather(context_key, 'sp', axis=0, tiled=True)  39.2 us
    all_gather x1, blocking collectives, body(): lax.all_gather(context_value, 'sp', axis=0, tiled=True)  37 us
    dynamic_slice x8, local copies, waits for them, and re-layouts, absorb_blocks(): carry, unused = lax.scan(step_block, carry, stacked)  22.7 us
    all_gather x3, blocking collectives, body(): shift, scale, gate = lax.all_gather(partial_mod, 'tp', axis=1, tiled=True)  22 us
    dot_general x3, matrix products, absorb(): jnp.einsum('kgts,skd->kgtd', terms.astype(jnp.bfloat16), value_heads, pre...  16.9 us
    reduce_sum x3, other arithmetic, absorb(): total = total * correction + jnp.sum(terms, axis=-1)  9.34 us
  transfers between devices with their start and end apart: 4, of which 3 were waited for; matrix products, arithmetic and copies ran while one was open for 5% of the time, Pallas kernels for 0%

commit v1 on v0

v1 whole, which is shorter than its diff:
```python
import functools
import math

import jax
import jax.numpy as jnp
from jax import lax
from jax.experimental import pallas as pl
from jax.experimental.pallas import tpu as pltpu
from jax.sharding import PartitionSpec as P

GRID_W = 64
EPS = 1e-06
F32 = jnp.float32
BF16 = jnp.bfloat16
MESH = pl.DeviceIdType.MESH


def kernel(
    sizes,
    latent,
    cond,
    ctx_cond,
    context,
    w_shift,
    w_scale,
    w_gate,
    pre_gain,
    post_gain,
    query_gain,
    key_gain,
    w_query,
    w_key,
    w_value,
    w_out,
    out,
    wq,
    wkv,
    wo,
    lat_all,
    mod_part,
    mod_recv,
    gate_part,
    gate_recv,
    mod_all,
    gate_all,
    xn,
    kv_send,
    cx_send,
    q_send,
    kvb,
    cxb,
    qb,
    m_ref,
    l_ref,
    acc_ref,
    att_send,
    att_recv,
    part_send,
    part_recv,
    w_sem,
    lat_ss,
    lat_rs,
    mp_ss,
    mp_rs,
    gp_ss,
    gp_rs,
    ma_ss,
    ma_rs,
    ga_ss,
    ga_rs,
    kva_ss,
    cxa_ss,
    kvz_ss,
    cxz_ss,
    kv_rs,
    cx_rs,
    q_ss,
    q_rs,
    at_ss,
    at_rs,
    pt_ss,
    pt_rs,
):
    n_sp, n_tp, fan, planes, group, hd, tok, rows, ctx = sizes
    width = w_shift.shape[1]
    depth = latent.shape[1]
    qw = group * hd
    me = lax.axis_index("sp")
    mt = lax.axis_index("tp")
    if fan == 1:
        f, g = 0, me
    else:
        f, g = lax.rem(me, fan), lax.div(me, fan)

    def remote(src, dst, ss, rs, **where):
        return pltpu.make_async_remote_copy(
            src_ref=src, dst_ref=dst, send_sem=ss, recv_sem=rs, device_id=where, device_id_type=MESH
        )

    loads = [pltpu.make_async_copy(w_query, wq, w_sem.at[0])]
    kv_loads = []
    for i in range(fan):
        cols = pl.ds(i * hd, hd)
        kv_loads.append(
            pltpu.make_async_copy(w_key.at[:, cols], wkv.at[i, :, pl.ds(0, hd)], w_sem.at[2 + 2 * i])
        )
        kv_loads.append(
            pltpu.make_async_copy(
                w_value.at[:, cols], wkv.at[i, :, pl.ds(hd, hd)], w_sem.at[3 + 2 * i]
            )
        )
    out_load = pltpu.make_async_copy(w_out, wo, w_sem.at[1])
    for copy in kv_loads + loads + [out_load]:
        copy.start()

    bar = pltpu.get_barrier_semaphore()

    @pl.loop(1, n_sp)
    def _(d):
        pl.semaphore_signal(
            bar, inc=1, device_id={"sp": lax.rem(me + d, n_sp)}, device_id_type=MESH
        )

    for d in range(1, n_tp):
        pl.semaphore_signal(
            bar, inc=1, device_id={"tp": lax.rem(mt + d, n_tp)}, device_id_type=MESH
        )

    def silu(v):
        v = v.astype(F32)
        return v / (1.0 + jnp.exp(-v))

    row_id = lax.broadcasted_iota(jnp.int32, (8, cond.shape[1]), 0)
    conds = jnp.where(
        row_id == 0, silu(cond[...]), jnp.where(row_id == 1, silu(ctx_cond[...]), 0.0)
    ).astype(BF16)
    part_shift = jnp.dot(conds, w_shift[...], preferred_element_type=F32)
    part_scale = jnp.dot(conds, w_scale[...], preferred_element_type=F32)
    part_gate = jnp.dot(conds, w_gate[...], preferred_element_type=F32)
    mod_part[0:2, :] = part_shift[0:2]
    mod_part[2:4, :] = part_scale[0:2]
    gate_part[...] = part_gate[0:1]
    pl.semaphore_wait(bar, n_sp - 1 + n_tp - 1)

    def mod_copy(d, slot):
        peer = lax.rem(me + d, n_sp)
        return remote(mod_part, mod_recv.at[slot], mp_ss.at[d], mp_rs.at[slot], sp=peer)

    def gate_copy(d, slot):
        peer = lax.rem(me + d, n_sp)
        return remote(gate_part, gate_recv.at[slot], gp_ss.at[d], gp_rs.at[slot], sp=peer)

    @pl.loop(1, n_sp)
    def _(d):
        mod_copy(d, me).start()

    def lat_copy(d, slot):
        peer = lax.rem(mt + d, n_tp)
        return remote(latent, lat_all.at[slot], lat_ss.at[d], lat_rs.at[slot], tp=peer)

    for d in range(1, n_tp):
        lat_copy(d, mt).start()

    @pl.loop(1, n_sp)
    def _(d):
        gate_copy(d, me).start()

    mod_recv[me] = mod_part[...]
    gate_recv[me] = gate_part[...]
    lat_all[mt] = latent[...]

    lane = lax.broadcasted_iota(jnp.int32, (tok, hd), 1)
    quarter = hd // 4
    pos = (me * tok + lax.broadcasted_iota(jnp.int32, (tok, hd), 0)).astype(F32)
    row_pos = jnp.floor(pos * (1.0 / GRID_W))
    col_pos = pos - row_pos * GRID_W
    step = (lane & (quarter - 1)).astype(F32)
    freq = jnp.exp(step * (-2.0 * math.log(10000.0) / (hd // 2)))
    angle = jnp.where(lane < hd // 2, row_pos, col_pos) * freq
    low = (lane & quarter) == 0
    cosine = jnp.cos(angle)
    sine = jnp.sin(angle)
    sine = jnp.where(low, -sine, sine)

    def head_rms(v, gain):
        return v * lax.rsqrt(jnp.mean(v * v, axis=-1, keepdims=True) + EPS) * gain

    def rotate(v):
        other = jnp.where(low, pltpu.roll(v, hd - quarter, 1), pltpu.roll(v, quarter, 1))
        return v * cosine + other * sine

    for d in range(1, n_tp):
        lat_copy(d, lax.rem(mt + d, n_tp)).wait_recv()

    def inverse(v):
        return lax.rsqrt(jnp.mean(v * v, axis=-1, keepdims=True) + EPS)

    lat_inv = [inverse(lat_all[t].astype(F32)) for t in range(n_tp)]
    ctx_inv = inverse(context[...].astype(F32))

    @pl.loop(1, n_sp)
    def _(d):
        mod_copy(d, lax.rem(me + d, n_sp)).wait_recv()

    total = lax.fori_loop(
        1, n_sp, lambda i, s: s + mod_recv[i], mod_recv[0]
    )
    mod_all[mt] = total

    def ma_copy(d, slot):
        peer = lax.rem(mt + d, n_tp)
        return remote(mod_all.at[mt], mod_all.at[slot], ma_ss.at[d], ma_rs.at[slot], tp=peer)

    for d in range(1, n_tp):
        ma_copy(d, mt).start()
    for d in range(1, n_tp):
        ma_copy(d, lax.rem(mt + d, n_tp)).wait_recv()

    for t in range(n_tp):
        cols = slice(t * width, (t + 1) * width)
        shift0, shift1 = mod_all[t, 0:1], mod_all[t, 1:2]
        scale0, scale1 = mod_all[t, 2:3], mod_all[t, 3:4]
        gain = pre_gain[:, cols]
        for s in range(n_tp):
            v = lat_all[s, :, cols].astype(F32) * lat_inv[s] * gain
            xn[s * rows : (s + 1) * rows, cols] = (v * (1.0 + scale0) + shift0).astype(BF16)
        v = context[:, cols].astype(F32) * ctx_inv * gain
        xn[tok : tok + ctx, cols] = (v * (1.0 + scale1) + shift1).astype(BF16)

    for copy in kv_loads:
        copy.wait()
    mine = pl.ds(pl.multiple_of(f * tok, tok), tok) if fan > 1 else pl.ds(0, tok)
    mine_c = pl.ds(pl.multiple_of(f * ctx, ctx), ctx) if fan > 1 else pl.ds(0, ctx)

    def block_rows(i):
        if fan == 1:
            return pl.ds(0, tok), pl.ds(0, ctx)
        return (
            pl.ds(pl.multiple_of(i * tok, tok), tok),
            pl.ds(pl.multiple_of(i * ctx, ctx), ctx),
        )

    def chip(plane, i):
        return plane * fan + i

    def project_kv(i):
        both = jnp.dot(xn[...], wkv[i], preferred_element_type=F32)
        k = head_rms(both[:, :hd], key_gain[...])
        v = both[:, hd:].astype(BF16)
        key = rotate(k[:tok]).astype(BF16)
        return key, v[:tok], k[tok:].astype(BF16), v[tok:]

    def kva_copy(i):
        return remote(
            kv_send.at[i], kvb.at[g, :, mine], kva_ss.at[i], kv_rs.at[me], sp=chip(g, i)
        )

    def cxa_copy(i):
        return remote(
            cx_send.at[i], cxb.at[g, :, mine_c], cxa_ss.at[i], cx_rs.at[me], sp=chip(g, i)
        )

    def kvz_copy(way, plane, i):
        r, rc = block_rows(i)
        src = chip(plane, i)
        peer = me + fan if way == 0 else me - fan
        return remote(
            kvb.at[plane, :, r], kvb.at[plane, :, r], kvz_ss.at[way, src], kv_rs.at[src], sp=peer
        )

    def cxz_copy(way, plane, i):
        r, rc = block_rows(i)
        src = chip(plane, i)
        peer = me + fan if way == 0 else me - fan
        return remote(
            cxb.at[plane, :, rc], cxb.at[plane, :, rc], cxz_ss.at[way, src], cx_rs.at[src], sp=peer
        )

    def pass_on(way, plane, i):
        room = g < planes - 1 if way == 0 else g > 0

        @pl.when(room)
        def _():
            kvz_copy(way, plane, i).start()
            cxz_copy(way, plane, i).start()

    def block_wait(plane, i):
        kvz_copy(0, plane, i).wait_recv()
        cxz_copy(0, plane, i).wait_recv()

    key, val, ckey, cval = project_kv(f)
    kvb[g, 0, mine] = key
    kvb[g, 1, mine] = val
    cxb[g, 0, mine_c] = ckey
    cxb[g, 1, mine_c] = cval
    pass_on(0, g, f)
    pass_on(1, g, f)
    for d in range(1, fan):
        i = lax.rem(f + d, fan)
        key, val, ckey, cval = project_kv(i)
        kv_send[i, 0] = key
        kv_send[i, 1] = val
        cx_send[i, 0] = ckey
        cx_send[i, 1] = cval
        kva_copy(i).start()
        cxa_copy(i).start()

    for copy in loads:
        copy.wait()

    def project_q(i):
        if fan == 1:
            w = wq[...]
        else:
            w = wq[:, pl.ds(pl.multiple_of(i * qw, qw), qw)]
        q = jnp.dot(xn[0:tok], w, preferred_element_type=F32)
        return [
            rotate(head_rms(q[:, h * hd : (h + 1) * hd], query_gain[...])).astype(BF16)
            for h in range(group)
        ]

    def q_copy(i, slot):
        return remote(q_send.at[i], qb.at[slot], q_ss.at[i], q_rs.at[slot], sp=chip(g, i))

    for d in range(1, fan):
        i = lax.rem(f + d, fan)
        for h, q in enumerate(project_q(i)):
            q_send[i, h] = q
        q_copy(i, f).start()
        j = lax.rem(f + fan - d, fan)
        block_wait(g, j)
        pass_on(0, g, j)
        pass_on(1, g, j)
    for h, q in enumerate(project_q(f)):
        qb[f, h] = q
    m_ref[...] = jnp.full(m_ref.shape, -1e30, F32)
    l_ref[...] = jnp.zeros(l_ref.shape, F32)
    acc_ref[...] = jnp.zeros(acc_ref.shape, F32)
    for d in range(1, fan):
        q_copy(f, lax.rem(f + d, fan)).wait_recv()

    root = math.sqrt(hd)
    lift = math.log(tok * n_sp / (4.0 * ctx * n_sp)) * root
    factor = math.log2(math.e) / root
    contract = (((1,), (1,)), ((), ()))

    def attend(plane):
        @pl.loop(0, fan)
        def _(i):
            for h in range(group):
                q = qb[i, h]
                s = lax.dot_general(q, kvb[plane, 0], contract, preferred_element_type=F32)
                c = lax.dot_general(q, cxb[plane, 0], contract, preferred_element_type=F32) + lift
                old = m_ref[i, h]
                new = jnp.maximum(
                    jnp.maximum(old, jnp.max(s, axis=-1, keepdims=True)),
                    jnp.max(c, axis=-1, keepdims=True),
                )
                fade = jnp.exp2((old - new) * factor)
                s = jnp.exp2((s - new) * factor)
                c = jnp.exp2((c - new) * factor)
                m_ref[i, h] = new
                l_ref[i, h] = (
                    l_ref[i, h] * fade
                    + jnp.sum(s, axis=-1, keepdims=True)
                    + jnp.sum(c, axis=-1, keepdims=True)
                )
                acc_ref[i, h] = (
                    acc_ref[i, h] * fade
                    + jnp.dot(s.astype(BF16), kvb[plane, 1], preferred_element_type=F32)
                    + jnp.dot(c.astype(BF16), cxb[plane, 1], preferred_element_type=F32)
                )

    attend(g)

    @pl.loop(1, planes)
    def _(t):
        for d in range(fan):
            i = lax.rem(f + fan - d, fan) if fan > 1 else 0

            @pl.when(g - t >= 0)
            def _():
                block_wait(g - t, i)
                pass_on(0, g - t, i)

            @pl.when(g + t < planes)
            def _():
                block_wait(g + t, i)
                pass_on(1, g + t, i)

        @pl.when(g - t >= 0)
        def _():
            attend(g - t)

        @pl.when(g + t < planes)
        def _():
            attend(g + t)

    def at_copy(i, slot):
        return remote(
            att_send.at[i], att_recv.at[slot], at_ss.at[i], at_rs.at[slot], sp=chip(g, i)
        )

    def attended(i):
        return [(acc_ref[i, h] / l_ref[i, h]).astype(BF16) for h in range(group)]

    for d in range(1, fan):
        i = lax.rem(f + d, fan)
        for h, a in enumerate(attended(i)):
            att_send[i, :, h * hd : (h + 1) * hd] = a
        at_copy(i, f).start()
    for h, a in enumerate(attended(f)):
        att_recv[f, :, h * hd : (h + 1) * hd] = a

    @pl.loop(1, n_sp)
    def _(d):
        gate_copy(d, lax.rem(me + d, n_sp)).wait_recv()

    gate_all[mt] = lax.fori_loop(1, n_sp, lambda i, s: s + gate_recv[i], gate_recv[0])

    def ga_copy(d, slot):
        peer = lax.rem(mt + d, n_tp)
        return remote(gate_all.at[mt], gate_all.at[slot], ga_ss.at[d], ga_rs.at[slot], tp=peer)

    for d in range(1, n_tp):
        ga_copy(d, mt).start()
    out_load.wait()
    for d in range(1, fan):
        at_copy(f, lax.rem(f + d, fan)).wait_recv()

    def project_out(t):
        r = pl.ds(pl.multiple_of(t * rows, rows), rows)
        wide = jnp.concatenate([att_recv[i, r] for i in range(fan)], axis=-1)
        return jnp.dot(wide, wo[...], preferred_element_type=F32).astype(BF16)

    def pt_copy(d, t, slot):
        return remote(part_send.at[t], part_recv.at[slot], pt_ss.at[t], pt_rs.at[slot], tp=t)

    for d in range(1, n_tp):
        t = lax.rem(mt + d, n_tp)
        part_send[t] = project_out(t)
        pt_copy(d, t, mt).start()
    part_recv[mt] = project_out(mt)
    for d in range(1, n_tp):
        ga_copy(d, lax.rem(mt + d, n_tp)).wait_recv()
    for d in range(1, n_tp):
        t = lax.rem(mt + d, n_tp)
        pt_copy(d, t, t).wait_recv()
    mixed = part_recv[0].astype(F32)
    for t in range(1, n_tp):
        mixed = mixed + part_recv[t].astype(F32)
    inv = lax.rsqrt(jnp.mean(mixed * mixed, axis=-1, keepdims=True) + EPS)
    for t in range(n_tp):
        cols = slice(t * width, (t + 1) * width)
        out[:, cols] = (
            latent[:, cols].astype(F32)
            + gate_all[t] * (mixed[:, cols] * inv * post_gain[:, cols])
        ).astype(BF16)

    @pl.loop(1, n_sp)
    def _(d):
        mod_copy(d, me).wait_send()
        gate_copy(d, me).wait_send()

    for d in range(1, n_tp):
        lat_copy(d, mt).wait_send()
        ma_copy(d, mt).wait_send()
        ga_copy(d, mt).wait_send()
        t = lax.rem(mt + d, n_tp)
        pt_copy(d, t, mt).wait_send()
    for d in range(1, fan):
        i = lax.rem(f + d, fan)
        kva_copy(i).wait_send()
        cxa_copy(i).wait_send()
        q_copy(i, f).wait_send()
        at_copy(i, f).wait_send()

    @pl.loop(0, planes)
    def _(plane):
        for i in range(fan):

            @pl.when((plane <= g) & (g < planes - 1))
            def _():
                kvz_copy(0, plane, i).wait_send()
                cxz_copy(0, plane, i).wait_send()

            @pl.when((plane >= g) & (g > 0))
            def _():
                kvz_copy(1, plane, i).wait_send()
                cxz_copy(1, plane, i).wait_send()


def body(
    latent,
    condition,
    context_condition,
    context,
    w_shift,
    w_scale,
    w_gate,
    pre_gain,
    post_gain,
    query_gain,
    key_gain,
    w_query,
    w_key,
    w_value,
    w_out,
):
    n_sp = lax.axis_size("sp")
    n_tp = lax.axis_size("tp")
    hd = query_gain.shape[0]
    kv_dev = w_key.shape[1] // hd
    group = w_query.shape[1] // w_key.shape[1]
    fan = kv_dev
    planes = n_sp // fan
    rows, depth = latent.shape
    tok = rows * n_tp
    ctx = context.shape[0]
    width = w_shift.shape[1]
    sizes = (n_sp, n_tp, fan, planes, group, hd, tok, rows, ctx)
    vmem = pl.BlockSpec(memory_space=pltpu.VMEM)
    hbm = pl.BlockSpec(memory_space=pl.ANY)
    dma = pltpu.SemaphoreType.DMA
    scratch = [
        pltpu.VMEM(w_query.shape, BF16),
        pltpu.VMEM((fan, depth, 2 * hd), BF16),
        pltpu.VMEM(w_out.shape, BF16),
        pltpu.VMEM((n_tp, rows, depth), BF16),
        pltpu.VMEM((4, width), F32),
        pltpu.VMEM((n_sp, 4, width), F32),
        pltpu.VMEM((1, width), F32),
        pltpu.VMEM((n_sp, 1, width), F32),
        pltpu.VMEM((n_tp, 4, width), F32),
        pltpu.VMEM((n_tp, 1, width), F32),
        pltpu.VMEM((tok + ctx, depth), BF16),
        pltpu.VMEM((fan, 2, tok, hd), BF16),
        pltpu.VMEM((fan, 2, ctx, hd), BF16),
        pltpu.VMEM((fan, group, tok, hd), BF16),
        pltpu.VMEM((planes, 2, fan * tok, hd), BF16),
        pltpu.VMEM((planes, 2, fan * ctx, hd), BF16),
        pltpu.VMEM((fan, group, tok, hd), BF16),
        pltpu.VMEM((fan, group, tok, 1), F32),
        pltpu.VMEM((fan, group, tok, 1), F32),
        pltpu.VMEM((fan, group, tok, hd), F32),
        pltpu.VMEM((fan, tok, group * hd), BF16),
        pltpu.VMEM((fan, tok, group * hd), BF16),
        pltpu.VMEM((n_tp, rows, depth), BF16),
        pltpu.VMEM((n_tp, rows, depth), BF16),
        dma((2 + 2 * fan,)),
        dma((n_tp,)),
        dma((n_tp,)),
        dma((n_sp,)),
        dma((n_sp,)),
        dma((n_sp,)),
        dma((n_sp,)),
        dma((n_tp,)),
        dma((n_tp,)),
        dma((n_tp,)),
        dma((n_tp,)),
        dma((fan,)),
        dma((fan,)),
        dma((2, n_sp)),
        dma((2, n_sp)),
        dma((n_sp,)),
        dma((n_sp,)),
        dma((fan,)),
        dma((fan,)),
        dma((fan,)),
        dma((fan,)),
        dma((n_tp,)),
        dma((n_tp,)),
    ]
    return pl.pallas_call(
        functools.partial(kernel, sizes),
        out_shape=jax.ShapeDtypeStruct(latent.shape, BF16),
        in_specs=[vmem] * 11 + [hbm] * 4,
        out_specs=vmem,
        scratch_shapes=scratch,
        compiler_params=pltpu.CompilerParams(
            collective_id=0, has_side_effects=True, vmem_limit_bytes=60 * 1024 * 1024
        ),
    )(
        latent,
        condition.reshape(1, -1),
        context_condition.reshape(1, -1),
        context,
        w_shift,
        w_scale,
        w_gate,
        pre_gain.reshape(1, -1),
        post_gain.reshape(1, -1),
        query_gain.reshape(1, -1),
        key_gain.reshape(1, -1),
        w_query,
        w_key,
        w_value,
        w_out,
    )


def solution(mesh):
    placed = (
        P(("sp", "tp"), None),
        P("sp"),
        P("sp"),
        P("sp", None),
        P("sp", "tp"),
        P("sp", "tp"),
        P("sp", "tp"),
        P(),
        P(),
        P(),
        P(),
        P(None, "tp"),
        P(None, "tp"),
        P(None, "tp"),
        P("tp", None),
    )
    return jax.shard_map(
        body, mesh=mesh, in_specs=placed, out_specs=P(("sp", "tp"), None), check_vma=False
    )
```

time: 350 us -> 89.3 us (0.26)
  blocking collectives: 162 us -> 0 us
  Pallas kernels: 0 us -> 87.2 us
  waiting for transfers between devices: 76.3 us -> 0 us
  matrix products: 43.9 us -> 0 us
  local copies, waits for them, and re-layouts: 28.5 us -> 1.88 us
  other arithmetic: 24.4 us -> 0 us
  between operations: 13.5 us -> 0.01 us
    all_gather x5 -> x0, blocking collectives: 98.2 us -> none  [the longest x1 39.2 us: body(): lax.all_gather(context_key, 'sp', axis=0, tiled=True)]
    pallas_call x0 -> x1, Pallas kernels: none -> 87.2 us  [body(): pl.pallas_call(functools.partial(kernel, sizes), out_shape=jax.ShapeDtype...]
    all_gather x3 -> x0, waiting for transfers between devices: 70.8 us -> none  [the longest x1 65.7 us: body(): lax.all_gather(key, 'sp', axis=0, tiled=True)]
    psum x1 -> x0, blocking collectives: 63.7 us -> none  [body(): partial_mod = lax.psum(partial_mod, 'sp')]
    dot_general x12 -> x0, matrix products: 43.9 us -> none  [the longest x3 16.9 us: absorb(): jnp.einsum('kgts,skd->kgtd', terms.astype(jnp.bfloat16), value_heads, pre...]
    dynamic_slice x8 -> x0, local copies, waits for them, and re-layouts: 22.7 us -> none  [absorb_blocks(): carry, unused = lax.scan(step_block, carry, stacked)]
    reduce_sum x9 -> x0, other arithmetic: 12.8 us -> none  [the longest x3 9.34 us: absorb(): total = total * correction + jnp.sum(terms, axis=-1)]
    reduce_scatter x1 -> x0, waiting for transfers between devices: 5.43 us -> none  [body(): lax.psum_scatter(jnp.dot(attended, w_out, preferred_element_type=jnp.floa...]
  transfers between devices with their start and end apart: 4 -> 0, of which waited for: 3 -> 0; matrix products, arithmetic and copies ran while one was open for 5% -> 0% of each run, Pallas kernels for 0% -> 0%
where the time goes in v1:
time: 89.3 us; the launch traced here: 89.1 us
  Pallas kernels  87.2 us (98%)
  local copies, waits for them, and re-layouts  1.88 us (2%)
    pallas_call x1, Pallas kernels, body(): pl.pallas_call(functools.partial(kernel, sizes), out_shape=jax.ShapeDtype...  87.2 us
    unnamed x1, local copies, waits for them, and re-layouts  1.88 us

profile of v1, /device:TPU:1, one launch (start us, length us, event | category | flops | bytes accessed | tf_op | source)
XLA Modules:
  0.0 89.1 jit_solution(3818401240226346471)
XLA Ops:
  0.0 87.2 %shard_map.145 = bf16[128,2048]{1,0:T(8,128)(2,1)} custom-call(bf16[128,2048]{1,0:T(8,128)(2,1)} %latent.1, bf16[1,128]{1,0:T(2,128)(2,1)} %bitcast.8, bf16[1,128]{1,0:T(2,128)(2,1)} %bitcast.9, bf16[32,2048]{1,0:T(8,128)(2,1)} %context.1, bf16[128,1024]{1,0:T(8,128)(2,1)} %w_shift.1, bf16[128,1024]{1,0:T(8,128)(2,1)} %w_scale.1, bf16[128,1024]{1,0:T(8,128)(2,1)} %w_gate.1, ...), custom_call_target="tpu_custom_call" | custom-call | tf_op jit(solution)/shard_map/pallas_call | solution.py:574
  87.2 1.9 %copy.17 = bf16[128,2048]{1,0:T(8,128)(2,1)} copy(bf16[128,2048]{1,0:T(8,128)(2,1)} %shard_map.145) | data formatting | bytes 1048576

commit v2 on v1

--- a/solution.py
+++ b/solution.py
@@ -336,65 +336,44 @@
     m_ref[...] = jnp.full(m_ref.shape, -1e30, F32)
     l_ref[...] = jnp.zeros(l_ref.shape, F32)
     acc_ref[...] = jnp.zeros(acc_ref.shape, F32)
-    for d in range(1, fan):
-        q_copy(f, lax.rem(f + d, fan)).wait_recv()
-
     root = math.sqrt(hd)
     lift = math.log(tok * n_sp / (4.0 * ctx * n_sp)) * root
     factor = math.log2(math.e) / root
     contract = (((1,), (1,)), ((), ()))
 
-    def attend(plane):
+    def absorb(i, key, value, ckey, cvalue):
+        for h in range(group):
+            q = qb[i, h]
+            s = lax.dot_general(q, key, contract, preferred_element_type=F32)
+            c = lax.dot_general(q, ckey, contract, preferred_element_type=F32) + lift
+            old = m_ref[i, h]
+            new = jnp.maximum(
+                jnp.maximum(old, jnp.max(s, axis=-1, keepdims=True)),
+                jnp.max(c, axis=-1, keepdims=True),
+            )
+            fade = jnp.exp2((old - new) * factor)
+            s = jnp.exp2((s - new) * factor)
+            c = jnp.exp2((c - new) * factor)
+            m_ref[i, h] = new
+            l_ref[i, h] = (
+                l_ref[i, h] * fade
+                + jnp.sum(s, axis=-1, keepdims=True)
+                + jnp.sum(c, axis=-1, keepdims=True)
+            )
+            acc_ref[i, h] = (
+                acc_ref[i, h] * fade
+                + jnp.dot(s.astype(BF16), value, preferred_element_type=F32)
+                + jnp.dot(c.astype(BF16), cvalue, preferred_element_type=F32)
+            )
+
+    def before(n):
+        return lax.rem(f + fan - n, fan) if fan > 1 else 0
+
+    def attend(plane, hook):
         @pl.loop(0, fan)
-        def _(i):
-            for h in range(group):
-                q = qb[i, h]
-                s = lax.dot_general(q, kvb[plane, 0], contract, preferred_element_type=F32)
-                c = lax.dot_general(q, cxb[plane, 0], contract, preferred_element_type=F32) + lift
-                old = m_ref[i, h]
-                new = jnp.maximum(
-                    jnp.maximum(old, jnp.max(s, axis=-1, keepdims=True)),
-                    jnp.max(c, axis=-1, keepdims=True),
-                )
-                fade = jnp.exp2((old - new) * factor)
-                s = jnp.exp2((s - new) * factor)
-                c = jnp.exp2((c - new) * factor)
-                m_ref[i, h] = new
-                l_ref[i, h] = (
-                    l_ref[i, h] * fade
-                    + jnp.sum(s, axis=-1, keepdims=True)
-                    + jnp.sum(c, axis=-1, keepdims=True)
-                )
-                acc_ref[i, h] = (
-                    acc_ref[i, h] * fade
-                    + jnp.dot(s.astype(BF16), kvb[plane, 1], preferred_element_type=F32)
-                    + jnp.dot(c.astype(BF16), cxb[plane, 1], preferred_element_type=F32)
-                )
-
-    attend(g)
-
-    @pl.loop(1, planes)
-    def _(t):
-        for d in range(fan):
-            i = lax.rem(f + fan - d, fan) if fan > 1 else 0
-
-            @pl.when(g - t >= 0)
-            def _():
-                block_wait(g - t, i)
-                pass_on(0, g - t, i)
-
-            @pl.when(g + t < planes)
-            def _():
-                block_wait(g + t, i)
-                pass_on(1, g + t, i)
-
-        @pl.when(g - t >= 0)
-        def _():
-            attend(g - t)
-
-        @pl.when(g + t < planes)
-        def _():
-            attend(g + t)
+        def _(n):
+            hook(n)
+            absorb(before(n), kvb[plane, 0], kvb[plane, 1], cxb[plane, 0], cxb[plane, 1])
 
     def at_copy(i, slot):
         return remote(
@@ -404,13 +383,96 @@
     def attended(i):
         return [(acc_ref[i, h] / l_ref[i, h]).astype(BF16) for h in range(group)]
 
-    for d in range(1, fan):
-        i = lax.rem(f + d, fan)
-        for h, a in enumerate(attended(i)):
-            att_send[i, :, h * hd : (h + 1) * hd] = a
-        at_copy(i, f).start()
-    for h, a in enumerate(attended(f)):
-        att_recv[f, :, h * hd : (h + 1) * hd] = a
+    def give(n, i):
+        @pl.when(n < fan - 1)
+        def _():
+            for h, a in enumerate(attended(i)):
+                att_send[i, :, h * hd : (h + 1) * hd] = a
+            at_copy(i, f).start()
+
+        @pl.when(n == fan - 1)
+        def _():
+            for h, a in enumerate(attended(f)):
+                att_recv[f, :, h * hd : (h + 1) * hd] = a
+
+    def after(n):
+        return lax.rem(f + 1 + n, fan) if fan > 1 else 0
+
+    top, bottom = g == planes - 1, g == 0
+    edge = top | bottom
+
+    def arrive(t, n):
+        i = before(n)
+
+        @pl.when((g - t >= 0) & (g < planes - 1))
+        def _():
+            block_wait(g - t, i)
+            pass_on(0, g - t, i)
+
+        @pl.when((g + t < planes) & (g > 0))
+        def _():
+            block_wait(g + t, i)
+            pass_on(1, g + t, i)
+
+    def first_hook(n):
+        if fan > 1:
+
+            @pl.when(n > 0)
+            def _():
+                q_copy(f, before(n)).wait_recv()
+
+        arrive(1, n)
+
+    attend(g, first_hook)
+
+    @pl.loop(1, planes - 1)
+    def _(t):
+        for n in range(fan):
+
+            @pl.when(top)
+            def _():
+                block_wait(g - t, before(n))
+
+            @pl.when(bottom)
+            def _():
+                block_wait(g + t, before(n))
+
+        @pl.when(g - t >= 0)
+        def _():
+            attend(g - t, lambda n: arrive(t + 1, n))
+
+        @pl.when((g + t < planes) & (g - t < 0))
+        def _():
+            attend(g + t, lambda n: arrive(t + 1, n))
+
+        @pl.when((g + t < planes) & (g - t >= 0))
+        def _():
+            attend(g + t, lambda n: None)
+
+    @pl.when(edge)
+    def _():
+        far = jnp.where(bottom, planes - 1, 0)
+
+        @pl.loop(0, fan)
+        def _(d):
+            j = before(d)
+            r, rc = block_rows(j)
+            block_wait(far, j)
+
+            @pl.loop(0, fan)
+            def _(n):
+                i = after(n)
+                absorb(i, kvb[far, 0, r], kvb[far, 1, r], cxb[far, 0, rc], cxb[far, 1, rc])
+
+                @pl.when(d == fan - 1)
+                def _():
+                    give(n, i)
+
+    @pl.when(jnp.logical_not(edge))
+    def _():
+        @pl.loop(0, fan)
+        def _(n):
+            give(n, after(n))
 
     @pl.loop(1, n_sp)
     def _(d):

time: 89.3 us -> 84.9 us (0.951)
  Pallas kernels: 87.2 us -> 82.8 us
    pallas_call x1, Pallas kernels: 87.2 us -> 82.8 us  [body(): pl.pallas_call(functools.partial(kernel, sizes), out_shape=jax.ShapeDtype...]
where the time goes in v2:
time: 84.9 us; the launch traced here: 84.7 us
  Pallas kernels  82.8 us (98%)
  local copies, waits for them, and re-layouts  1.88 us (2%)
    pallas_call x1, Pallas kernels, body(): pl.pallas_call(functools.partial(kernel, sizes), out_shape=jax.ShapeDtype...  82.8 us
    unnamed x1, local copies, waits for them, and re-layouts  1.88 us

profile of v2, /device:TPU:1, one launch (start us, length us, event | category | flops | bytes accessed | tf_op | source)
XLA Modules:
  0.0 84.7 jit_solution(2265781392547271535)
XLA Ops:
  0.0 82.8 %shard_map.145 = bf16[128,2048]{1,0:T(8,128)(2,1)} custom-call(bf16[128,2048]{1,0:T(8,128)(2,1)} %latent.1, bf16[1,128]{1,0:T(2,128)(2,1)} %bitcast.8, bf16[1,128]{1,0:T(2,128)(2,1)} %bitcast.9, bf16[32,2048]{1,0:T(8,128)(2,1)} %context.1, bf16[128,1024]{1,0:T(8,128)(2,1)} %w_shift.1, bf16[128,1024]{1,0:T(8,128)(2,1)} %w_scale.1, bf16[128,1024]{1,0:T(8,128)(2,1)} %w_gate.1, ...), custom_call_target="tpu_custom_call" | custom-call | tf_op jit(solution)/shard_map/pallas_call | solution.py:636
  82.8 1.9 %copy.17 = bf16[128,2048]{1,0:T(8,128)(2,1)} copy(bf16[128,2048]{1,0:T(8,128)(2,1)} %shard_map.145) | data formatting | bytes 1048576

commit v3 on v2

--- a/solution.py
+++ b/solution.py
@@ -110,7 +110,7 @@
             )
         )
     out_load = pltpu.make_async_copy(w_out, wo, w_sem.at[1])
-    for copy in kv_loads + loads + [out_load]:
+    for copy in kv_loads:
         copy.start()
 
     bar = pltpu.get_barrier_semaphore()
@@ -161,9 +161,8 @@
     for d in range(1, n_tp):
         lat_copy(d, mt).start()
 
-    @pl.loop(1, n_sp)
-    def _(d):
-        gate_copy(d, me).start()
+    for copy in loads + [out_load]:
+        copy.start()
 
     mod_recv[me] = mod_part[...]
     gate_recv[me] = gate_part[...]
@@ -333,6 +332,10 @@
         pass_on(1, g, j)
     for h, q in enumerate(project_q(f)):
         qb[f, h] = q
+    @pl.loop(1, n_sp)
+    def _(d):
+        gate_copy(d, me).start()
+
     m_ref[...] = jnp.full(m_ref.shape, -1e30, F32)
     l_ref[...] = jnp.zeros(l_ref.shape, F32)
     acc_ref[...] = jnp.zeros(acc_ref.shape, F32)

time: 84.9 us -> 85.2 us (level)
  no operation moved by 1% of the time
where the time goes in v3:
time: 85.2 us; the launch traced here: 85.1 us
  Pallas kernels  83.2 us (98%)
  local copies, waits for them, and re-layouts  1.88 us (2%)
    pallas_call x1, Pallas kernels, body(): pl.pallas_call(functools.partial(kernel, sizes), out_shape=jax.ShapeDtype...  83.2 us
    unnamed x1, local copies, waits for them, and re-layouts  1.88 us

profile of v3, /device:TPU:1, one launch (start us, length us, event | category | flops | bytes accessed | tf_op | source)
XLA Modules:
  0.0 85.1 jit_solution(17624963900880440530)
XLA Ops:
  0.0 83.2 %shard_map.145 = bf16[128,2048]{1,0:T(8,128)(2,1)} custom-call(bf16[128,2048]{1,0:T(8,128)(2,1)} %latent.1, bf16[1,128]{1,0:T(2,128)(2,1)} %bitcast.8, bf16[1,128]{1,0:T(2,128)(2,1)} %bitcast.9, bf16[32,2048]{1,0:T(8,128)(2,1)} %context.1, bf16[128,1024]{1,0:T(8,128)(2,1)} %w_shift.1, bf16[128,1024]{1,0:T(8,128)(2,1)} %w_scale.1, bf16[128,1024]{1,0:T(8,128)(2,1)} %w_gate.1, ...), custom_call_target="tpu_custom_call" | custom-call | tf_op jit(solution)/shard_map/pallas_call | solution.py:639
  83.2 1.9 %copy.17 = bf16[128,2048]{1,0:T(8,128)(2,1)} copy(bf16[128,2048]{1,0:T(8,128)(2,1)} %shard_map.145) | data formatting | bytes 1048576
